TPU v7x, 512 devices: a whole 4x4x16 slice. The times are simulated.
512 devices in a mesh: sp: 16 (over z), dp: 32 (over y, x, core).
Axes of the slice: x: 4, y: 4, z: 16, core: 2. Of those that a mesh axis runs over, the one named last changes fastest.
Arguments:
- queries: bfloat16 [32, 3072, 16, 128], P('dp', 'sp'), may hold values from -6 to 6
- keys: bfloat16 [32, 3072, 16, 128], P('dp', 'sp'), may hold values from -6 to 6
- values: bfloat16 [32, 3072, 16, 128], P('dp', 'sp'), may hold values from -6 to 6
- mix_ratio: float32 [16], replicated, may hold values from 0.3 to 0.8
- out_gain: float32 [128], replicated, may hold values from 0.1 to 1.9
- out_weight: bfloat16 [2048, 2048], P(None, 'dp'), may hold values from -0.125 to 0.125
Outputs:
- layer_out: bfloat16 [32, 3072, 2048], P('dp', 'sp')
All inputs are finite; a program needn't handle non-finite values.
Results may differ from a plain program's by a relative error of at most 0.0098.
Values may be sent and summed in bfloat16 or wider, within the bound.
No kernel may reach another device: no remote copies, remote signals or barrier semaphores. Data moves between devices by JAX's collectives and lax.ppermute only.
A program may use at most 64 MiB of HBM per device.

v0:
```python
import math

import jax
import jax.numpy as jnp
from jax import lax
from jax.sharding import PartitionSpec as P

theta_base = 500000.0
neg_large = -1e30
norm_eps = 1e-05


def in_one_piece(arrays, axis, split_dim, concat_dim, along):
    ends, at = ([], 0)
    for a in arrays[:-1]:
        at += a.shape[along]
        ends.append(at)
    both = jnp.concatenate(arrays, axis=along)
    return tuple(
        jnp.split(
            lax.all_to_all(both, axis, split_axis=split_dim, concat_axis=concat_dim, tiled=True),
            ends,
            axis=along,
        )
    )


def cut_along(array, dim, peers):
    before, after = (array.shape[:dim], array.shape[dim + 1 :])
    return jnp.moveaxis(array.reshape(*before, peers, -1, *after), dim, 0)


def piece_ends(length, count):
    turn = length // count
    if turn >= 8:
        turn -= turn % 8
    return [turn * k for k in range(1, count)]


def in_order(blocks, dim):
    dims = list(blocks.shape[1:])
    dims[dim] *= blocks.shape[0]
    return jnp.moveaxis(blocks, 0, dim).reshape(dims)


def exchange_in_pieces(array, axis, pieces, split_dim, concat_dim):
    blocks = cut_along(array, split_dim, lax.axis_size(axis))
    cut = max(range(1, max(2, blocks.ndim - 1)), key=lambda d: blocks.shape[d])
    outs = []
    for section in jnp.split(blocks, piece_ends(blocks.shape[cut], pieces), axis=cut):
        if section.size:
            outs.append(lax.all_to_all(section, axis, split_axis=0, concat_axis=0, tiled=True))
    return in_order(jnp.concatenate(outs, axis=cut), concat_dim)


def rotate_halves(field, positions):
    width = field.shape[-1] // 2
    half = width // 2
    freqs = theta_base ** (-jnp.arange(half, dtype=jnp.float32) * 2.0 / width)
    angle = positions.astype(jnp.float32)[:, None] * freqs[None, :]
    cosine = jnp.cos(angle)[:, None, :]
    sine = jnp.sin(angle)[:, None, :]
    parts = field.reshape(field.shape[0], 2, width)
    lower = parts[..., :half]
    upper = parts[..., half:]
    turned = jnp.concatenate(
        [lower * cosine - upper * sine, upper * cosine + lower * sine], axis=-1
    )
    return turned.reshape(field.shape)


def masked_softmax(scores, visible):
    kept = jnp.where(visible, scores, neg_large)
    highest = jnp.max(kept, axis=-1, keepdims=True)
    powers = jnp.exp(kept - highest)
    return powers / jnp.sum(powers, axis=-1, keepdims=True)


def head_attention(query_head, key_head, value_head, ratio, gain):
    length = query_head.shape[0]
    width = query_head.shape[1] // 2
    positions = jnp.arange(length, dtype=jnp.int32)
    rotated_queries = (
        rotate_halves(query_head.astype(jnp.float32), positions) * width ** (-0.5)
    ).astype(jnp.bfloat16)
    rotated_keys = rotate_halves(key_head.astype(jnp.float32), positions).astype(jnp.bfloat16)
    block = math.gcd(512, length)

    def one_block(start):
        query_rows = lax.dynamic_slice_in_dim(rotated_queries, start, block, 0)
        visible = (start + jnp.arange(block, dtype=jnp.int32))[:, None] >= positions[None, :]
        first = jnp.dot(
            query_rows[:, :width], rotated_keys[:, :width].T, preferred_element_type=jnp.float32
        )
        second = jnp.dot(
            query_rows[:, width:], rotated_keys[:, width:].T, preferred_element_type=jnp.float32
        )
        weights = (masked_softmax(first, visible) - ratio * masked_softmax(second, visible)).astype(
            jnp.bfloat16
        )
        mixed = jnp.dot(weights, value_head, preferred_element_type=jnp.float32)
        scale = lax.rsqrt(jnp.mean(mixed * mixed, axis=-1, keepdims=True) + norm_eps)
        return (mixed * scale * gain).astype(jnp.bfloat16)

    starts = jnp.arange(length // block, dtype=jnp.int32) * block
    return lax.map(one_block, starts).reshape(length, value_head.shape[1])


def on_device(queries, keys, values, mix_ratio, out_gain, out_weight):
    groups = lax.axis_size("sp")
    heads_here = queries.shape[2] // groups
    query_all, key_all, value_all = in_one_piece((queries, keys, values), "sp", 2, 1, 0)
    seqs = query_all.shape[0]
    length = query_all.shape[1]
    first_head = lax.axis_index("sp") * heads_here
    ratios = lax.dynamic_slice_in_dim(mix_ratio, first_head, heads_here, 0)
    item_ratios = jnp.tile(ratios, seqs)

    def by_item(field):
        return jnp.swapaxes(field, 1, 2).reshape(seqs * heads_here, length, field.shape[3])

    def one_head(head_items):
        query_head, key_head, value_head, ratio = head_items
        return head_attention(query_head, key_head, value_head, ratio, out_gain)

    heads = lax.map(
        one_head, (by_item(query_all), by_item(key_all), by_item(value_all), item_ratios)
    )
    attended = jnp.swapaxes(heads.reshape(seqs, heads_here, length, heads.shape[2]), 1, 2)
    returned = exchange_in_pieces(attended, "sp", 2, 1, 2)
    tokens_here = returned.shape[1]
    token_rows = returned.reshape(seqs * tokens_here, -1)
    result = jnp.dot(
        token_rows,
        lax.all_gather(out_weight, "dp", axis=1, tiled=True),
        preferred_element_type=jnp.float32,
    ).astype(jnp.bfloat16)
    return result.reshape(seqs, tokens_here, -1)


def solution(mesh):
    in_specs = (
        P("dp", "sp", None, None),
        P("dp", "sp", None, None),
        P("dp", "sp", None, None),
        P(),
        P(),
        P(None, "dp"),
    )
    out_specs = P("dp", "sp", None)
    return jax.shard_map(
        on_device, mesh=mesh, in_specs=in_specs, out_specs=out_specs, check_vma=False
    )
```

profile of v0, /device:TPU:6, one launch (start us, length us, event | category | flops | bytes accessed | tf_op | source)
XLA Modules:
  0.0 304.8 jit_solution(9597755954184421023)
XLA Ops:
  6.5 1.3 copy.15
  7.9 1.3 copy.16
  9.2 1.3 copy.17
  10.6 1.7 pad_maximum_fusion
  12.3 15.2 %all-to-all-start = ((bf16[3,192,16,128]{3,1,0,2:T(8,128)(2,1)}), bf16[3,192,16,128]{3,1,0,2:T(8,128)(2,1)S(1)}, u32[]{:S(2)}, u32[]{:S(2)}) async-start(bf16[3,192,16,128]{3,1,0,2:T(8,128)(2,1)} %pad_maximum_fusion), calls=%async_computation | async-start | bytes 4718592 | tf_op jit(solution)/shard_map/all_to_all | solution.py:21
  27.6 0.7 all-gather.2.cloned.1.call-update
  28.9 1.4 multiply_cosine_fusion
  30.3 103.8 %all-to-all-done = bf16[3,192,16,128]{3,1,0,2:T(8,128)(2,1)S(1)} async-done(((bf16[3,192,16,128]{3,1,0,2:T(8,128)(2,1)}), bf16[3,192,16,128]{3,1,0,2:T(8,128)(2,1)S(1)}, u32[]{:S(2)}, u32[]{:S(2)}) %all-to-all-start) | async-done | bytes 2359328 | tf_op jit(solution)/shard_map/all_to_all | solution.py:21
  134.1 2.1 fusion.19
  136.2 2.1 copy.18
  138.4 2.0 reshape.110
  140.3 2.1 copy.19
  142.5 2.1 reshape.111
  144.6 2.2 subtract_convert_fusion.2
  147.4 80.6 %while.18 = (s32[]{:T(128)}, bf16[6,512,128]{2,1,0:T(8,128)(2,1)}, s32[6]{0:T(128)S(1)}, bf16[3072,128]{0,1:T(8,128)(2,1)S(1)}, bf16[3072,128]{1,0:T(8,128)(2,1)...) while((s32[]{:T(128)}, bf16[6,512,128]{2,1,0:T(8,128)(2,1)}, ...), condition=%wide.region_6.7_spmd.clone, body=%wide.region_0.6_spmd.clone.sunk | while | flops 832371712 | bytes 44600544 | solution.py:106
  150.5 1.9 fusion.29
  152.3 1.7 fusion.28
  154.0 2.1 fusion.30
  156.1 3.8 %multiply_reduce_fusion.2 = (f32[512]{0:T(512)S(1)}, f32[512,128]{0,1:T(8,128)S(1)}) fusion(bf16[3072,128]{1,0:T(8,128)(2,1)S(1)} %copy-done, f32[512,3072]{1,0:T(8,128)S(1)} %get-tuple-element.202, f32[512,3072]{1,0:T(8,128)S(1)} %get-tuple-element.203, f32[512]{0:T(512)S(1)} %get-tuple-element.206, f32[512]{0:T(512)S(1)} %get-tuple-element.205, ...), kind=kOutput, calls=%fused_computation.13.clone.1 | convolution fusion | flops 413793792 | bytes 13641732 | tf_op jit(solution)/shard_map/while/body/eval_jaxpr/while/body/eval_jaxpr/dot_general | solution.py:101
  160.1 0.7 constant_dynamic-update-slice_fusion.2
  163.9 1.9 fusion.29
  165.8 1.7 fusion.28
  167.5 2.1 fusion.30
  169.6 3.8 %multiply_reduce_fusion.2 = (f32[512]{0:T(512)S(1)}, f32[512,128]{0,1:T(8,128)S(1)}) fusion(bf16[3072,128]{1,0:T(8,128)(2,1)S(1)} %copy-done, f32[512,3072]{1,0:T(8,128)S(1)} %get-tuple-element.202, f32[512,3072]{1,0:T(8,128)S(1)} %get-tuple-element.203, f32[512]{0:T(512)S(1)} %get-tuple-element.206, f32[512]{0:T(512)S(1)} %get-tuple-element.205, ...), kind=kOutput, calls=%fused_computation.13.clone.1 | convolution fusion | flops 413793792 | bytes 13641732 | tf_op jit(solution)/shard_map/while/body/eval_jaxpr/while/body/eval_jaxpr/dot_general | solution.py:101
  173.6 0.7 constant_dynamic-update-slice_fusion.2
  177.3 1.9 fusion.29
  179.2 1.7 fusion.28
  180.9 2.1 fusion.30
  183.0 3.8 %multiply_reduce_fusion.2 = (f32[512]{0:T(512)S(1)}, f32[512,128]{0,1:T(8,128)S(1)}) fusion(bf16[3072,128]{1,0:T(8,128)(2,1)S(1)} %copy-done, f32[512,3072]{1,0:T(8,128)S(1)} %get-tuple-element.202, f32[512,3072]{1,0:T(8,128)S(1)} %get-tuple-element.203, f32[512]{0:T(512)S(1)} %get-tuple-element.206, f32[512]{0:T(512)S(1)} %get-tuple-element.205, ...), kind=kOutput, calls=%fused_computation.13.clone.1 | convolution fusion | flops 413793792 | bytes 13641732 | tf_op jit(solution)/shard_map/while/body/eval_jaxpr/while/body/eval_jaxpr/dot_general | solution.py:101
  187.0 0.7 constant_dynamic-update-slice_fusion.2
  190.8 1.9 fusion.29
  192.6 1.7 fusion.28
  194.3 2.1 fusion.30
  196.4 3.8 %multiply_reduce_fusion.2 = (f32[512]{0:T(512)S(1)}, f32[512,128]{0,1:T(8,128)S(1)}) fusion(bf16[3072,128]{1,0:T(8,128)(2,1)S(1)} %copy-done, f32[512,3072]{1,0:T(8,128)S(1)} %get-tuple-element.202, f32[512,3072]{1,0:T(8,128)S(1)} %get-tuple-element.203, f32[512]{0:T(512)S(1)} %get-tuple-element.206, f32[512]{0:T(512)S(1)} %get-tuple-element.205, ...), kind=kOutput, calls=%fused_computation.13.clone.1 | convolution fusion | flops 413793792 | bytes 13641732 | tf_op jit(solution)/shard_map/while/body/eval_jaxpr/while/body/eval_jaxpr/dot_general | solution.py:101
  204.2 1.9 fusion.29
  206.1 1.7 fusion.28
  207.8 2.1 fusion.30
  209.9 3.8 %multiply_reduce_fusion.2 = (f32[512]{0:T(512)S(1)}, f32[512,128]{0,1:T(8,128)S(1)}) fusion(bf16[3072,128]{1,0:T(8,128)(2,1)S(1)} %copy-done, f32[512,3072]{1,0:T(8,128)S(1)} %get-tuple-element.202, f32[512,3072]{1,0:T(8,128)S(1)} %get-tuple-element.203, f32[512]{0:T(512)S(1)} %get-tuple-element.206, f32[512]{0:T(512)S(1)} %get-tuple-element.205, ...), kind=kOutput, calls=%fused_computation.13.clone.1 | convolution fusion | flops 413793792 | bytes 13641732 | tf_op jit(solution)/shard_map/while/body/eval_jaxpr/while/body/eval_jaxpr/dot_general | solution.py:101
  213.9 0.7 constant_dynamic-update-slice_fusion.2
  217.6 1.9 fusion.29
  219.5 1.7 fusion.28
  221.2 2.1 fusion.30
  223.3 3.8 %multiply_reduce_fusion.2 = (f32[512]{0:T(512)S(1)}, f32[512,128]{0,1:T(8,128)S(1)}) fusion(bf16[3072,128]{1,0:T(8,128)(2,1)S(1)} %copy-done, f32[512,3072]{1,0:T(8,128)S(1)} %get-tuple-element.202, f32[512,3072]{1,0:T(8,128)S(1)} %get-tuple-element.203, f32[512]{0:T(512)S(1)} %get-tuple-element.206, f32[512]{0:T(512)S(1)} %get-tuple-element.205, ...), kind=kOutput, calls=%fused_computation.13.clone.1 | convolution fusion | flops 413793792 | bytes 13641732 | tf_op jit(solution)/shard_map/while/body/eval_jaxpr/while/body/eval_jaxpr/dot_general | solution.py:101
  227.3 0.7 constant_dynamic-update-slice_fusion.2
  228.0 1.2 slice_bitcast_fusion.1
  229.1 31.4 %all_to_all.25 = bf16[16,1,96,1,128]{4,2,3,1,0:T(8,128)(2,1)S(1)} all-to-all(bf16[16,1,96,1,128]{4,2,3,1,0:T(8,128)(2,1)S(1)} %get-tuple-element.139), channel_id=1, replica_groups=mesh['sp'=16,'dp'=32] {'sp'}, dimensions={0} | all-to-all | bytes 786432 | tf_op jit(solution)/shard_map/all_to_all | solution.py:52
  260.5 29.6 %all_to_all.26 = bf16[16,1,96,1,128]{4,2,3,1,0:T(8,128)(2,1)S(1)} all-to-all(bf16[16,1,96,1,128]{4,2,3,1,0:T(8,128)(2,1)S(1)} %get-tuple-element.140), channel_id=1, replica_groups=mesh['sp'=16,'dp'=32] {'sp'}, dimensions={0} | all-to-all | bytes 786432 | tf_op jit(solution)/shard_map/all_to_all | solution.py:52
  290.8 7.2 %fusion.13 = bf16[1,192,2048]{2,1,0:T(8,128)(2,1)} fusion(bf16[2048,2048]{0,1:T(8,128)(2,1)} %all-gather.2.cloned.1.call-done, bf16[24,8,16,128]{3,2,1,0:T(8,128)(2,1)S(1)} %bitcast.46), kind=kOutput, calls=%fused_computation.22 | convolution fusion | flops 1611005952 | bytes 9961472 | tf_op jit(solution)/shard_map/dot_general | solution.py:133
  (59 shorter events, 11.1 us)
Async XLA Ops:
  7.9 20.4 %copy-start.2 = (f32[16]{0:T(128)S(1)}, f32[16]{0:T(128)}, u32[]{:S(2)}) copy-start(f32[16]{0:T(128)} %param.11) | copy-start | bytes 196
  12.3 121.8 %all-to-all-start = ((bf16[3,192,16,128]{3,1,0,2:T(8,128)(2,1)}), bf16[3,192,16,128]{3,1,0,2:T(8,128)(2,1)S(1)}, u32[]{:S(2)}, u32[]{:S(2)}) async-start(bf16[3,192,16,128]{3,1,0,2:T(8,128)(2,1)} %pad_maximum_fusion), calls=%async_computation | async-start | bytes 4718592 | tf_op jit(solution)/shard_map/all_to_all | solution.py:21
  27.5 263.3 %all-gather.2.cloned.1.call-start = ((), (), s32[]{:S(2)}) async-start(), calls=%async_computation.3 | async-start | bytes 8650752 | tf_op jit(solution)/shard_map/all_gather | solution.py:135
  144.6 2.8 copy-start.1
  154.0 2.1 copy-start
  167.5 2.1 copy-start
  180.9 2.1 copy-start
  194.3 2.1 copy-start
  207.8 2.1 copy-start
  221.2 2.1 copy-start
Sparse Core Ops, SparseCore 0:
  31.5 69.2 all-gather.1
where the time goes:
time: 305 us
  waiting for transfers between devices  105 us (34%)
  blocking collectives  61 us (20%)
  matrix products  51.1 us (17%)
  other arithmetic  24.6 us (8%)
  local copies, waits for them, and re-layouts  23.3 us (8%)
  starting transfers between devices  15.2 us (5%)
  between operations  13.5 us (4%)
  loops' own time  11.5 us (4%)
    all_to_all x1, waiting for transfers between devices, in_one_piece(): lax.all_to_all(both, axis, split_axis=split_dim, concat_axis=concat_dim,...  104 us
    all_to_all x2, blocking collectives, exchange_in_pieces(): lax.all_to_all(section, axis, split_axis=0, concat_axis=0, tiled=True)  61 us
    dot_general x6, matrix products, one_block(): mixed = jnp.dot(weights, value_head, preferred_element_type=jnp.float32)  22.5 us
    all_to_all x1, starting transfers between devices, in_one_piece(): lax.all_to_all(both, axis, split_axis=split_dim, concat_axis=concat_dim,...  15.2 us
    reduce_sum x6, other arithmetic, masked_softmax(): return powers / jnp.sum(powers, axis=-1, keepdims=True)  12.5 us
    another operation x1, loops' own time, head_attention(): return lax.map(one_block, starts).reshape(length, value_head.shape[1])  11.5 us
    dot_general x6, matrix products, one_block(): jnp.dot(query_rows[:, width:], rotated_keys[:, width:].T, preferred_eleme...  11.2 us
    dot_general x6, matrix products, one_block(): jnp.dot(query_rows[:, :width], rotated_keys[:, :width].T, preferred_eleme...  10.3 us
  transfers between devices with their start and end apart: 2, of which 1 were waited for; matrix products, arithmetic and copies ran while one was open for 28% of the time, Pallas kernels for 0%

commit v1 on v0

v1 whole, which is shorter than its diff:
```python
import functools

import jax
import jax.numpy as jnp
import numpy as np
from jax import lax
from jax.experimental import pallas as pl
from jax.experimental.pallas import tpu as pltpu
from jax.sharding import PartitionSpec as P

theta_base = 500000.0
neg_large = -1e30
norm_eps = 1e-05
TILE = 256


def turn_kernel(base_ref, freq_ref, q_ref, k_ref, out_ref):
    tokens, heads, width = q_ref.shape
    lane = lax.broadcasted_iota(jnp.int32, (tokens, width), 1)
    row = lax.broadcasted_iota(jnp.int32, (tokens, width), 0)
    first = base_ref[0] + pl.program_id(0) * tokens
    angle = (first + row).astype(jnp.float32) * freq_ref[...]
    lower = lane % 64 < 32
    cosine = jnp.cos(angle)[:, None, :]
    sine = jnp.where(lower, -jnp.sin(angle), jnp.sin(angle))[:, None, :]
    lower = jnp.broadcast_to(lower[:, None, :], (tokens, heads, width))

    def turned(x):
        flat = x.reshape(tokens * heads, width)
        up = pltpu.roll(flat, width - 32, 1).reshape(tokens, heads, width)
        down = pltpu.roll(flat, 32, 1).reshape(tokens, heads, width)
        return x * cosine + jnp.where(lower, up, down) * sine

    q = turned(q_ref[...].astype(jnp.float32)) * 0.125
    out_ref[:, 0] = jnp.swapaxes(q, 0, 1).astype(jnp.bfloat16)
    k = turned(k_ref[...].astype(jnp.float32))
    out_ref[:, 1] = jnp.swapaxes(k, 0, 1).astype(jnp.bfloat16)


def turn_and_group(q, k, first_position):
    tokens, heads, width = q.shape
    step = 48
    lanes = np.arange(width) % 32
    freqs = jnp.asarray((theta_base ** (-lanes * 2.0 / 64.0)).astype(np.float32)[None, :])
    block = pl.BlockSpec((step, heads, width), lambda i: (i, 0, 0))
    return pl.pallas_call(
        turn_kernel,
        name="turn",
        grid=(tokens // step,),
        in_specs=[
            pl.BlockSpec(memory_space=pltpu.SMEM),
            pl.BlockSpec((1, width), lambda i: (0, 0)),
            block,
            block,
        ],
        out_specs=pl.BlockSpec((heads, 2, step, width), lambda i: (0, 0, i, 0)),
        out_shape=jax.ShapeDtypeStruct((heads, 2, tokens, width), jnp.bfloat16),
    )(first_position, freqs, q, k)


def weights_kernel(ratio_ref, qk_ref, out_ref, q_s, k_s, s_s, m_s, l_s):
    planes, _, tokens, width = qk_ref.shape
    blocks = planes * tokens // TILE
    step = pl.program_id(0)

    @pl.when(step == 0)
    def _():
        for z in range(planes):
            q_s[z * tokens : (z + 1) * tokens, :] = qk_ref[z, 0]
            k_s[z * tokens : (z + 1) * tokens, :] = qk_ref[z, 1]

    ratio = ratio_ref[0]

    def one_row(row, at):
        q = q_s[pl.ds(pl.multiple_of(row * TILE, TILE), TILE), :]
        lane = lax.broadcasted_iota(jnp.int32, (TILE, width), 1)
        zero = jnp.zeros_like(q)
        both = jnp.concatenate([jnp.where(lane < 64, q, zero), jnp.where(lane < 64, zero, q)], axis=0)

        def tile_scores(j):
            keys = k_s[pl.ds(pl.multiple_of(j * TILE, TILE), TILE), :]
            return lax.dot_general(
                both, keys, (((1,), (1,)), ((), ())), preferred_element_type=jnp.float32
            )

        r = lax.broadcasted_iota(jnp.int32, (2 * TILE, TILE), 0)
        c = lax.broadcasted_iota(jnp.int32, (2 * TILE, TILE), 1)
        s = jnp.where(r % TILE >= c, tile_scores(row), neg_large)
        s_s[row] = s
        m_s[...] = jnp.maximum(s[:, :128], s[:, 128:])

        @pl.loop(0, row)
        def _(j):
            s = tile_scores(j)
            s_s[j] = s
            m_s[...] = jnp.maximum(m_s[...], jnp.maximum(s[:, :128], s[:, 128:]))

        top = jnp.max(m_s[...], axis=-1, keepdims=True)
        m_s[...] = jnp.broadcast_to(top, m_s.shape)
        l_s[...] = jnp.zeros_like(l_s)

        @pl.loop(0, row + 1)
        def _(j):
            s = s_s[j]
            m = m_s[...]
            e0 = jnp.exp(s[:, :128] - m)
            e1 = jnp.exp(s[:, 128:] - m)
            l_s[...] += e0 + e1
            s_s[j] = jnp.concatenate([e0, e1], axis=1)

        total = jnp.sum(l_s[...], axis=-1, keepdims=True)
        a1 = 1.0 / total[:TILE]
        a2 = ratio / total[TILE:]
        l_s[...] = jnp.broadcast_to(jnp.concatenate([a1, a2], axis=0), l_s.shape)

        @pl.loop(0, row + 1)
        def _(j):
            b1 = l_s[:TILE, :]
            b2 = l_s[TILE:, :]
            e = s_s[j]
            w0 = e[:TILE, :128] * b1 - e[TILE:, :128] * b2
            w1 = e[:TILE, 128:] * b1 - e[TILE:, 128:] * b2
            out_ref[0, at + j] = jnp.concatenate([w0, w1], axis=1).astype(jnp.bfloat16)

    one_row(step, 0)
    one_row(blocks - 1 - step, step + 1)


def attention_weights(ratio, qk):
    planes, _, tokens, width = qk.shape
    blocks = planes * tokens // TILE
    return pl.pallas_call(
        weights_kernel,
        name="weights",
        grid=(blocks // 2,),
        in_specs=[
            pl.BlockSpec(memory_space=pltpu.SMEM),
            pl.BlockSpec(qk.shape, lambda p: (0, 0, 0, 0)),
        ],
        out_specs=pl.BlockSpec((1, blocks + 1, TILE, TILE), lambda p: (p, 0, 0, 0)),
        out_shape=jax.ShapeDtypeStruct((blocks // 2, blocks + 1, TILE, TILE), jnp.bfloat16),
        scratch_shapes=[
            pltpu.VMEM((planes * tokens, width), jnp.bfloat16),
            pltpu.VMEM((planes * tokens, width), jnp.bfloat16),
            pltpu.VMEM((blocks, 2 * TILE, TILE), jnp.float32),
            pltpu.VMEM((2 * TILE, 128), jnp.float32),
            pltpu.VMEM((2 * TILE, 128), jnp.float32),
        ],
        cost_estimate=pl.CostEstimate(
            flops=8 * 10**9, bytes_accessed=14 * 10**6, transcendentals=10**7
        ),
    )(ratio, qk)


def mix_kernel(gain_ref, w_ref, v_ref, out_ref, v_s, o_s):
    planes, tokens, width = v_ref.shape
    blocks = planes * tokens // TILE
    step = pl.program_id(0)

    @pl.when(step == 0)
    def _():
        for z in range(planes):
            v_s[z * tokens : (z + 1) * tokens, :] = v_ref[z]

    def one_row(row, at):
        def add(j, acc):
            vals = v_s[pl.ds(pl.multiple_of(j * TILE, TILE), TILE), :]
            return acc + jnp.dot(w_ref[0, at + j], vals, preferred_element_type=jnp.float32)

        mixed = lax.fori_loop(0, row + 1, add, jnp.zeros((TILE, width), jnp.float32))
        scale = lax.rsqrt(jnp.mean(mixed * mixed, axis=-1, keepdims=True) + norm_eps)
        o_s[pl.ds(pl.multiple_of(row * TILE, TILE), TILE), :] = (
            mixed * scale * gain_ref[...]
        ).astype(jnp.bfloat16)

    one_row(step, 0)
    one_row(blocks - 1 - step, step + 1)

    @pl.when(step == blocks // 2 - 1)
    def _():
        for z in range(planes):
            out_ref[z] = o_s[z * tokens : (z + 1) * tokens, :]


def mix_values(gain, w, v):
    planes, tokens, width = v.shape
    blocks = planes * tokens // TILE
    whole = pl.BlockSpec(v.shape, lambda p: (0, 0, 0))
    return pl.pallas_call(
        mix_kernel,
        name="mix",
        grid=(blocks // 2,),
        in_specs=[
            pl.BlockSpec((1, width), lambda p: (0, 0)),
            pl.BlockSpec((1, blocks + 1, TILE, TILE), lambda p: (p, 0, 0, 0)),
            whole,
        ],
        out_specs=whole,
        out_shape=jax.ShapeDtypeStruct(v.shape, jnp.bfloat16),
        scratch_shapes=[
            pltpu.VMEM((planes * tokens, width), jnp.bfloat16),
            pltpu.VMEM((planes * tokens, width), jnp.bfloat16),
        ],
    )(gain, w, v)


def project_kernel(a_ref, w_ref, out_ref, a_s):
    heads, tokens, width = a_ref.shape

    @pl.when(pl.program_id(0) == 0)
    def _():
        for h in range(heads):
            a_s[:, h * width : (h + 1) * width] = a_ref[h]

    out_ref[...] = lax.dot_general(
        a_s[...], w_ref[...], (((1,), (1,)), ((), ())), preferred_element_type=jnp.float32
    ).astype(jnp.bfloat16)


def project(attended, weight_rows):
    heads, tokens, width = attended.shape
    columns = weight_rows.shape[0]
    step = 256
    return pl.pallas_call(
        project_kernel,
        name="project",
        grid=(columns // step,),
        in_specs=[
            pl.BlockSpec(attended.shape, lambda c: (0, 0, 0)),
            pl.BlockSpec((step, heads * width), lambda c: (c, 0)),
        ],
        out_specs=pl.BlockSpec((tokens, step), lambda c: (0, c)),
        out_shape=jax.ShapeDtypeStruct((tokens, columns), jnp.bfloat16),
        scratch_shapes=[pltpu.VMEM((tokens, heads * width), jnp.bfloat16)],
    )(attended, weight_rows)


def exchange(array):
    return lax.all_to_all(array, "sp", split_axis=0, concat_axis=0, tiled=True)


def on_device(queries, keys, values, mix_ratio, out_gain, out_weight):
    place = lax.axis_index("sp")
    tokens = queries.shape[1]
    first_position = (place * tokens).astype(jnp.int32).reshape(1)
    ratio = lax.dynamic_slice_in_dim(mix_ratio, place, 1, 0)
    weight_rows = lax.all_gather(out_weight.T, "dp", axis=0, tiled=True)
    qk = exchange(turn_and_group(queries[0], keys[0], first_position))
    by_head = jnp.swapaxes(values[0], 0, 1)
    by_head, qk = lax.optimization_barrier((by_head, qk))
    v = exchange(by_head)
    w = attention_weights(ratio, qk)
    attended = exchange(mix_values(out_gain[None, :], w, v))
    return project(attended, weight_rows)[None]


def solution(mesh):
    tokens = P("dp", "sp", None, None)
    return jax.shard_map(
        on_device,
        mesh=mesh,
        in_specs=(tokens, tokens, tokens, P(), P(), P(None, "dp")),
        out_specs=P("dp", "sp", None),
        check_vma=False,
    )
```

time: 305 us -> 232 us (0.76)
  Pallas kernels: 0 us -> 67.3 us
  matrix products: 51.1 us -> 0 us
  waiting for transfers between devices: 105 us -> 75.6 us
  other arithmetic: 24.6 us -> 0 us
  local copies, waits for them, and re-layouts: 23.3 us -> 3.71 us
  loops' own time: 11.5 us -> 0 us
  blocking collectives: 61 us -> 50.1 us
  starting transfers between devices: 15.2 us -> 21.3 us
    pallas_call x0 -> x4, Pallas kernels: none -> 67.3 us  [the longest x1 35.6 us: attention_weights(): pl.pallas_call(weights_kernel, name='weights', grid=(blocks // 2,), in_sp...]
    dot_general x19 -> x0, matrix products: 51.1 us -> none  [the longest x6 22.5 us: one_block(): mixed = jnp.dot(weights, value_head, preferred_element_type=jnp.float32)]
    all_to_all x1 -> x2, waiting for transfers between devices: 104 us -> 74.9 us  [exchange(): return lax.all_to_all(array, 'sp', split_axis=0, concat_axis=0, tiled=True)]
    reduce_sum x6 -> x0, other arithmetic: 12.5 us -> none  [masked_softmax(): return powers / jnp.sum(powers, axis=-1, keepdims=True)]
    another operation x1 -> x0, loops' own time: 11.5 us -> none  [head_attention(): return lax.map(one_block, starts).reshape(length, value_head.shape[1])]
    all_to_all x2 -> x1, blocking collectives: 61 us -> 50.1 us  [exchange(): return lax.all_to_all(array, 'sp', split_axis=0, concat_axis=0, tiled=True)]
    convert_element_type x4 -> x0, local copies, waits for them, and re-layouts: 8.32 us -> none  [the longest x2 4.2 us: head_attention(): key_head.astype(jnp.float32)]
    all_to_all x1 -> x2, starting transfers between devices: 15.2 us -> 21.3 us  [exchange(): return lax.all_to_all(array, 'sp', split_axis=0, concat_axis=0, tiled=True)]
  transfers between devices with their start and end apart: 2 -> 3, of which waited for: 1 -> 2; matrix products, arithmetic and copies ran while one was open for 28% -> 1% of each run, Pallas kernels for 0% -> 25%
where the time goes in v1:
time: 232 us; the launch traced here: 231 us
  waiting for transfers between devices  75.6 us (33%)
  Pallas kernels  67.3 us (29%)
  blocking collectives  50.1 us (22%)
  starting transfers between devices  21.3 us (9%)
  between operations  13.4 us (6%)
  local copies, waits for them, and re-layouts  3.71 us (2%)
    all_to_all x2, waiting for transfers between devices, exchange(): return lax.all_to_all(array, 'sp', split_axis=0, concat_axis=0, tiled=True)  74.9 us
    all_to_all x1, blocking collectives, exchange(): return lax.all_to_all(array, 'sp', split_axis=0, concat_axis=0, tiled=True)  50.1 us
    pallas_call x1, Pallas kernels, attention_weights(): pl.pallas_call(weights_kernel, name='weights', grid=(blocks // 2,), in_sp...  35.6 us
    all_to_all x2, starting transfers between devices, exchange(): return lax.all_to_all(array, 'sp', split_axis=0, concat_axis=0, tiled=True)  21.3 us
    pallas_call x1, Pallas kernels, mix_values(): pl.pallas_call(mix_kernel, name='mix', grid=(blocks // 2,), in_specs=[pl....  18 us
    pallas_call x1, Pallas kernels, project(): pl.pallas_call(project_kernel, name='project', grid=(columns // step,), i...  8.98 us
    pallas_call x1, Pallas kernels, turn_and_group(): pl.pallas_call(turn_kernel, name='turn', grid=(tokens // step,), in_specs...  4.73 us
  transfers between devices with their start and end apart: 3, of which 2 were waited for; matrix products, arithmetic and copies ran while one was open for 1% of the time, Pallas kernels for 25%

profile of v1, /device:TPU:6, one launch (start us, length us, event | category | flops | bytes accessed | tf_op | source)
XLA Modules:
  0.0 231.4 jit_solution(18280285804518744710)
XLA Ops:
  6.5 0.0 copy-start.2
  6.5 0.0 all-gather.2.cloned.1.call-start
  6.5 0.7 all-gather.2.cloned.1.call-update
  7.3 4.7 %turn.1 = bf16[16,2,192,128]{3,2,1,0:T(8,128)(2,1)} custom-call(s32[1]{0:T(128)} %bitcast.3.base_ref, f32[1,128]{1,0:T(1,128)} %constant.14.clone.freq_ref, bf16[192,16,128]{2,1,0:T(8,128)(2,1)} %bitcast.11, bf16[192,16,128]{2,1,0:T(8,128)(2,1)} %bitcast.12), custom_call_target="tpu_custom_call" | custom-call | tf_op jit(solution)/shard_map/turn/pallas_call | solution.py:46
  12.0 15.2 %all-to-all-start = ((bf16[16,2,192,128]{3,2,1,0:T(8,128)(2,1)}), bf16[16,2,192,128]{3,2,1,0:T(8,128)(2,1)S(1)}, u32[]{:S(2)}, u32[]{:S(2)}) async-start(bf16[16,2,192,128]{3,2,1,0:T(8,128)(2,1)} %turn.1), calls=%async_computation | async-start | bytes 3145728 | tf_op jit(solution)/shard_map/all_to_all | solution.py:239
  27.2 2.2 copy.10
  29.4 72.0 %all-to-all-done.qk_ref = bf16[16,2,192,128]{3,2,1,0:T(8,128)(2,1)S(1)} async-done(((bf16[16,2,192,128]{3,2,1,0:T(8,128)(2,1)}), bf16[16,2,192,128]{3,2,1,0:T(8,128)(2,1)S(1)}, u32[]{:S(2)}, u32[]{:S(2)}) %all-to-all-start) | async-done | bytes 1572896 | tf_op jit(solution)/shard_map/all_to_all | solution.py:239
  101.4 0.0 copy-start.1
  101.4 6.1 %all-to-all-start.1 = ((bf16[16,192,128]{2,1,0:T(8,128)(2,1)}), bf16[16,192,128]{2,1,0:T(8,128)(2,1)S(1)}, u32[]{:S(2)}, u32[]{:S(2)}) async-start(bf16[16,192,128]{2,1,0:T(8,128)(2,1)} %bitcast.10), calls=%async_computation.1 | async-start | bytes 1572864 | tf_op jit(solution)/shard_map/all_to_all | solution.py:239
  107.5 0.0 copy-done.2
  107.5 0.6 dynamic_slice.3.ratio_ref
  108.1 0.0 copy-done.1
  108.1 35.6 %weights.1.w_ref = bf16[6,13,256,256]{3,2,1,0:T(8,128)(2,1)} custom-call(f32[1]{0:T(128)} %dynamic_slice.3.ratio_ref, bf16[16,2,192,128]{3,2,1,0:T(8,128)(2,1)} %copy-done.1), custom_call_target="tpu_custom_call" | custom-call | flops 8000000000 | bytes 14000000 | tf_op jit(solution)/shard_map/weights/pallas_call | solution.py:132
  143.7 2.9 %all-to-all-done.1.v_ref = bf16[16,192,128]{2,1,0:T(8,128)(2,1)S(1)} async-done(((bf16[16,192,128]{2,1,0:T(8,128)(2,1)}), bf16[16,192,128]{2,1,0:T(8,128)(2,1)S(1)}, u32[]{:S(2)}, u32[]{:S(2)}) %all-to-all-start.1) | async-done | bytes 786464 | tf_op jit(solution)/shard_map/all_to_all | solution.py:239
  146.6 0.0 copy-start
  146.6 0.9 copy-done
  147.5 18.0 %mix.1 = bf16[16,192,128]{2,1,0:T(8,128)(2,1)} custom-call(f32[1,128]{1,0:T(1,128)} %bitcast.14, bf16[6,13,256,256]{3,2,1,0:T(8,128)(2,1)} %weights.1.w_ref, bf16[16,192,128]{2,1,0:T(8,128)(2,1)} %copy-done), custom_call_target="tpu_custom_call" | custom-call | tf_op jit(solution)/shard_map/mix/pallas_call | solution.py:189
  165.5 50.1 %all_to_all.15.a_ref = bf16[16,192,128]{2,1,0:T(8,128)(2,1)} all-to-all(bf16[16,192,128]{2,1,0:T(8,128)(2,1)} %mix.1), channel_id=1, replica_groups=mesh['sp'=16,'dp'=32] {'sp'}, dimensions={0} | all-to-all | bytes 1572864 | tf_op jit(solution)/shard_map/all_to_all | solution.py:239
  215.6 0.0 all-gather.2.cloned.1.call-done.w_ref
  215.6 9.0 %project.1 = bf16[192,2048]{1,0:T(8,128)(2,1)} custom-call(bf16[16,192,128]{2,1,0:T(8,128)(2,1)} %all_to_all.15.a_ref, bf16[2048,2048]{1,0:T(8,128)(2,1)} %all-gather.2.cloned.1.call-done.w_ref), custom_call_target="tpu_custom_call" | custom-call | tf_op jit(solution)/shard_map/project/pallas_call | solution.py:224
Async XLA Ops:
  6.5 101.0 %copy-start.2 = (f32[16]{0:T(128)S(1)}, f32[16]{0:T(128)}, u32[]{:S(2)}) copy-start(f32[16]{0:T(128)} %param.10) | copy-start | bytes 196
  6.5 209.0 %all-gather.2.cloned.1.call-start = ((), (), s32[]{:S(2)}) async-start(), calls=%async_computation.3 | async-start | bytes 8650752 | tf_op jit(solution)/shard_map/all_gather | solution.py:247
  12.0 89.4 %all-to-all-start = ((bf16[16,2,192,128]{3,2,1,0:T(8,128)(2,1)}), bf16[16,2,192,128]{3,2,1,0:T(8,128)(2,1)S(1)}, u32[]{:S(2)}, u32[]{:S(2)}) async-start(bf16[16,2,192,128]{3,2,1,0:T(8,128)(2,1)} %turn.1), calls=%async_computation | async-start | bytes 3145728 | tf_op jit(solution)/shard_map/all_to_all | solution.py:239
  101.4 6.7 %copy-start.1 = (bf16[16,2,192,128]{3,2,1,0:T(8,128)(2,1)}, bf16[16,2,192,128]{3,2,1,0:T(8,128)(2,1)S(1)}, u32[]{:S(2)}) copy-start(bf16[16,2,192,128]{3,2,1,0:T(8,128)(2,1)S(1)} %all-to-all-done.qk_ref) | copy-start | bytes 4718596
  101.4 45.2 %all-to-all-start.1 = ((bf16[16,192,128]{2,1,0:T(8,128)(2,1)}), bf16[16,192,128]{2,1,0:T(8,128)(2,1)S(1)}, u32[]{:S(2)}, u32[]{:S(2)}) async-start(bf16[16,192,128]{2,1,0:T(8,128)(2,1)} %bitcast.10), calls=%async_computation.1 | async-start | bytes 1572864 | tf_op jit(solution)/shard_map/all_to_all | solution.py:239
  146.6 0.9 copy-start
Sparse Core Ops, SparseCore 0:
  10.5 72.3 all-gather.1
